TPU v7x, 256 devices: a whole 4x4x8 slice. The times are simulated.
256 devices in a mesh: sp: 16 (over y, x), dp: 16 (over z, core).
Axes of the slice: x: 4, y: 4, z: 8, core: 2. Of those that a mesh axis runs over, the one named last changes fastest.
Arguments:
- value_half: bfloat16 [16, 4096, 2048], P('dp', 'sp'), may hold values from -6 to 6
- gate_half: bfloat16 [16, 4096, 2048], P('dp', 'sp'), may hold values from -6 to 6
- upstream: bfloat16 [16, 4096, 2048], P('dp', 'sp'), may hold values from -6 to 6
- conv_taps: float32 [31, 2048], P(None, 'sp'), may hold values from -1 to 1
- norm_gain: float32 [2048], replicated, may hold values from 0.1 to 1.9
- out_weight: bfloat16 [2048, 2048], P('dp'), may hold values from -0.125 to 0.125
Outputs:
- grad_value: bfloat16 [16, 4096, 2048], P('dp', 'sp')
- grad_gate: bfloat16 [16, 4096, 2048], P('dp', 'sp')
- grad_taps: float32 [31, 2048], P(None, 'sp')
- grad_gain: float32 [2048], replicated
- grad_weight: float32 [2048, 2048], P('dp')
All inputs are finite; a program needn't handle non-finite values.
Results may differ from a plain program's by a relative error of at most 0.0062.
Values may be sent and summed in bfloat16 or wider, within the bound.
A program may use at most 128 MiB of HBM per device.

v0:
```python
import functools
import jax
import jax.numpy as jnp
from jax import lax
from jax.sharding import Mesh
from jax.sharding import PartitionSpec as P

DP = ("dp_0", "dp_1")
SP = ("sp_0", "sp_1")
SP_DP = ("sp_0", "sp_1", "dp_0", "dp_1")
NORM_EPS = 1e-05


def from_everyone(shard, axis):
    count = lax.axis_size(axis)
    return lax.all_to_all(
        jnp.broadcast_to(shard[None], (count, *shard.shape)), axis, 0, 0, tiled=True
    )


def of_everyone(shard, axis):
    return from_everyone(shard, axis).sum(axis=0)


def one_axis_at_a_time(shard, axes):
    return functools.reduce(lax.psum, axes, shard)


def body(value_half, gate_half, upstream, conv_taps, norm_gain, out_weight):
    tap_count = conv_taps.shape[0]
    sig_gate = jax.nn.sigmoid(gate_half.astype(jnp.float32))
    value_wide = value_half.astype(jnp.float32)
    glu = (value_wide * sig_gate).astype(jnp.bfloat16)
    glu_heads = lax.all_to_all(glu, SP, split_axis=2, concat_axis=1, tiled=True).astype(jnp.float32)
    length = glu_heads.shape[1]
    padded = jnp.pad(glu_heads, ((0, 0), (tap_count - 1, 0), (0, 0)))
    conv_out = jnp.zeros_like(glu_heads)
    for offset in range(tap_count):
        conv_out = conv_out + conv_taps[offset] * padded[:, offset : offset + length]
    conv_tokens = lax.all_to_all(
        conv_out.astype(jnp.bfloat16), SP, split_axis=1, concat_axis=2, tiled=True
    ).astype(jnp.float32)
    row_mean = jnp.mean(conv_tokens, axis=-1, keepdims=True)
    centered = conv_tokens - row_mean
    inv_scale = lax.rsqrt(jnp.mean(centered * centered, axis=-1, keepdims=True) + NORM_EPS)
    normed = centered * inv_scale
    scaled = normed * norm_gain
    sig_scaled = jax.nn.sigmoid(scaled)
    activated = (scaled * sig_scaled).astype(jnp.bfloat16)[0]
    upstream_rows = upstream[0]
    columns = upstream_rows
    grad_act = jnp.dot(
        columns,
        lax.all_gather(out_weight, DP, axis=0, tiled=True),
        preferred_element_type=jnp.float32,
    )
    grad_scaled = grad_act[None] * sig_scaled * (1.0 + scaled * (1.0 - sig_scaled))
    gain_part = jnp.sum(grad_scaled * normed, axis=(0, 1))
    grad_normed = grad_scaled * norm_gain
    grad_conv_out = inv_scale * (
        grad_normed
        - jnp.mean(grad_normed, axis=-1, keepdims=True)
        - normed * jnp.mean(grad_normed * normed, axis=-1, keepdims=True)
    )
    grad_heads = lax.all_to_all(
        grad_conv_out.astype(jnp.bfloat16), SP, split_axis=2, concat_axis=1, tiled=True
    ).astype(jnp.float32)
    grad_padded = jnp.pad(grad_heads, ((0, 0), (0, tap_count - 1), (0, 0)))
    grad_glu = jnp.zeros_like(grad_heads)
    tap_terms = []
    for offset in range(tap_count):
        first = tap_count - 1 - offset
        grad_glu = grad_glu + conv_taps[offset] * grad_padded[:, first : first + length]
        tap_terms.append(jnp.sum(grad_heads * padded[:, offset : offset + length], axis=(0, 1)))
    grad_taps = of_everyone(jnp.stack(tap_terms), DP)
    grad_tokens = lax.all_to_all(
        grad_glu.astype(jnp.bfloat16), SP, split_axis=1, concat_axis=2, tiled=True
    ).astype(jnp.float32)
    grad_value = (grad_tokens * sig_gate).astype(jnp.bfloat16)
    grad_gate = (grad_tokens * value_wide * sig_gate * (1.0 - sig_gate)).astype(jnp.bfloat16)
    grad_gain = one_axis_at_a_time(gain_part, SP_DP)
    columns = upstream_rows
    owned = lax.psum_scatter(
        lax.dot_general(
            columns, activated, (((0,), (0,)), ((), ())), preferred_element_type=jnp.float32
        ),
        DP,
        scatter_dimension=0,
        tiled=True,
    )
    grad_weight = lax.psum(owned, SP)
    return (grad_value, grad_gate, grad_taps, grad_gain, grad_weight)


def solution(mesh):
    torus = Mesh(mesh.devices.reshape(4, 4, 8, 2), ("sp_0", "sp_1", "dp_0", "dp_1"))
    placed = (P(DP, SP, None), P(DP, SP, None), P(DP, SP, None), P(None, SP), P(), P(DP, None))
    return jax.shard_map(
        body,
        mesh=torus,
        in_specs=placed,
        out_specs=(P(DP, SP, None), P(DP, SP, None), P(None, SP), P(), P(DP, None)),
        check_vma=False,
    )
```

profile of v0, /device:TPU:32, one launch (start us, length us, event | category | flops | bytes accessed | tf_op | source)
XLA Modules:
  0.0 445.5 jit_solution(18143520017637400832)
XLA Ops:
  9.4 1.9 copy.76
  11.9 12.9 %copy.120 = bf16[1,256,2048]{1,0,2:T(2,128)(2,1)} copy(bf16[1,256,2048]{1,2,0:T(8,128)(2,1)S(1)} %fusion.1) | data formatting | bytes 2097152 | tf_op jit(solution)/shard_map/convert_element_type | solution.py:33
  25.3 11.6 %reduce.17 = bf16[2048,256]{1,0:T(8,128)(2,1)S(1)} reduce(bf16[2048,1,256]{2,1,0:T(2,128)(2,1)} %bitcast.226, bf16[]{:T(256)} %broadcast.202), dimensions={1}, to_apply=%bitcast.207.reduce_sub_computation | reduce | bytes 2097154
  38.1 7.1 %all-to-all-start = ((bf16[16,2,16384]{2,1,0:T(2,128)(2,1)}), bf16[16,2,16384]{2,1,0:T(2,128)(2,1)}, u32[]{:S(2)}, u32[]{:S(2)}) async-start(bf16[16,2,16384]{2,1,0:T(2,128)(2,1)} %reshape.390), calls=%async_computation | async-start | bytes 2097152 | tf_op jit(solution)/shard_map/all_to_all | solution.py:34
  45.5 17.5 %all-to-all-done = bf16[16,2,16384]{2,1,0:T(2,128)(2,1)} async-done(((bf16[16,2,16384]{2,1,0:T(2,128)(2,1)}), bf16[16,2,16384]{2,1,0:T(2,128)(2,1)}, u32[]{:S(2)}, u32[]{:S(2)}) %all-to-all-start) | async-done | bytes 1048608 | tf_op jit(solution)/shard_map/all_to_all | solution.py:34
  62.9 4.3 reshape.391
  67.2 1.6 copy_convert_fusion.2
  69.2 1.9 copy.79
  71.1 8.6 %add_convert_fusion.1 = bf16[1,4096,128]{2,1,0:T(8,128)(2,1)S(1)} fusion(f32[128]{0:T(128)S(1)} %get-tuple-element.104, f32[128]{0:T(128)S(1)} %get-tuple-element.105, f32[128]{0:T(128)S(1)} %get-tuple-element.76, f32[128]{0:T(128)S(1)} %get-tuple-element.77, f32[128]{0:T(128)S(1)} %get-tuple-element.78, f32[128]{0:T(128)S(1)} %get-tuple-element.79, ...), kind=kLoop, calls=%fused_computation.83 | loop fusion | flops 32505856 | bytes 5258752 | tf_op jit(solution)/shard_map/convert_element_type | solution.py:41
  79.7 17.1 %copy.119 = bf16[1,4096,128]{2,0,1:T(2,128)(2,1)} copy(bf16[1,4096,128]{2,1,0:T(8,128)(2,1)S(1)} %add_convert_fusion.1) | data formatting | bytes 2097152 | tf_op jit(solution)/shard_map/convert_element_type | solution.py:41
  96.7 24.4 %reduce.18 = bf16[4096,128]{1,0:T(8,128)(2,1)} reduce(bf16[4096,1,128]{2,1,0:T(2,128)(2,1)} %bitcast.228, bf16[]{:T(256)} %broadcast.202), dimensions={1}, to_apply=%bitcast.206.reduce_sub_computation | reduce | bytes 2097154
  121.1 2.1 reshape.392
  123.2 20.4 %all_to_all.20 = bf16[16,2,16384]{2,1,0:T(2,128)(2,1)} all-to-all(bf16[16,2,16384]{2,1,0:T(2,128)(2,1)} %reshape.392), channel_id=1, replica_groups=mesh['sp_0'=4,'sp_1'=4,'dp_0'=8,'dp_1'=2] {'sp_0','sp_1'}, dimensions={0} | all-to-all | bytes 2097152 | tf_op jit(solution)/shard_map/all_to_all | solution.py:40
  143.6 5.8 %reshape.393 = bf16[4096,1,128]{2,1,0:T(2,128)(2,1)} reshape(bf16[16,2,16384]{2,1,0:T(2,128)(2,1)} %all_to_all.20) | data formatting | bytes 2097152
  149.4 2.2 fusion.33
  151.6 3.0 copy_convert_fusion.1
  154.6 2.9 copy.82
  157.6 2.0 fusion.11
  159.8 1.8 fusion.29
  161.6 2.3 copy.91
  163.9 9.3 %convolution_bitcast_fusion = f32[2048,2048]{0,1:T(8,128)} fusion(bf16[256,2048]{0,1:T(8,128)(2,1)} %bitcast.233, bf16[1,256,2048]{2,1,0:T(8,128)(2,1)S(1)} %copy-done), kind=kOutput, calls=%fused_computation | convolution fusion | flops 2147483648 | bytes 18874368 | tf_op jit(solution)/shard_map/dot_general | solution.py:84
  173.2 4.2 copy.83
  177.4 7.7 %multiply_reduce_fusion = (f32[2048]{0:T(1024)S(1)}, f32[256]{0:T(256)S(1)}, f32[256]{0:T(256)S(1)}, f32[256,2048]{1,0:T(8,128)S(1)}) fusion(f32[256]{0:T(256)S(1)} %add_rsqrt_fusion, f32[256]{0:T(256)S(1)} %broadcast_multiply_fusion.2, f32[32,8,16,128]{3,2,1,0:T(8,128)} %bitcast.224, f32[2048]{0:T(1024)S(1)} %copy-done.10, ...), kind=kOutput, calls=%fused_computation.22 | convolution fusion | flops 2156393984 | bytes 13651968 | tf_op jit(solution)/shard_map/dot_general | solution.py:52
  186.1 3.8 copy.84
  189.9 12.1 %reduce.19 = bf16[2048,256]{1,0:T(8,128)(2,1)S(1)} reduce(bf16[2048,1,256]{2,1,0:T(2,128)(2,1)} %bitcast.229, bf16[]{:T(256)} %broadcast.202), dimensions={1}, to_apply=%bitcast.194.reduce_sub_computation | reduce | bytes 2097154
  203.1 18.8 %all_to_all.42 = bf16[16,2,16384]{2,1,0:T(2,128)(2,1)S(1)} all-to-all(bf16[16,2,16384]{2,1,0:T(2,128)(2,1)} %reshape.394), channel_id=1, replica_groups=mesh['sp_0'=4,'sp_1'=4,'dp_0'=8,'dp_1'=2] {'sp_0','sp_1'}, dimensions={0} | all-to-all | bytes 2097152 | tf_op jit(solution)/shard_map/all_to_all | solution.py:65
  221.9 3.5 reshape.395
  225.3 3.1 copy_convert_fusion
  228.4 2.9 copy.86
  231.4 2.8 multiply_reduce_fusion.1
  235.2 2.5 multiply_reduce_fusion.2
  237.7 2.5 multiply_reduce_fusion.4
  240.2 2.5 multiply_reduce_fusion.3
  243.6 8.5 %all-to-all-start.4 = ((f32[16,31,128]{2,1,0:T(8,128)}), f32[16,31,128]{2,1,0:T(8,128)S(1)}, u32[]{:S(2)}, u32[]{:S(2)}) async-start(f32[16,31,128]{2,1,0:T(8,128)} %broadcast_in_dim.2), calls=%async_computation.4 | async-start | bytes 524288 | tf_op jit(solution)/shard_map/all_to_all | solution.py:16
  252.1 37.3 %add_convert_fusion = bf16[1,4096,128]{2,1,0:T(8,128)(2,1)S(1)} fusion(f32[1,4096,128]{2,1,0:T(8,128)} %bitcast.213, f32[128]{0:T(128)S(1)} %get-tuple-element.104, f32[128]{0:T(128)S(1)} %get-tuple-element.105, f32[128]{0:T(128)S(1)} %get-tuple-element.76, f32[128]{0:T(128)S(1)} %get-tuple-element.77, f32[128]{0:T(128)S(1)} %get-tuple-element.78, ...), kind=kLoop, calls=%fused_computation.54 | loop fusion | flops 32505856 | bytes 3161600 | tf_op jit(solution)/shard_map/convert_element_type | solution.py:77
  289.4 16.7 %copy.118 = bf16[1,4096,128]{2,0,1:T(2,128)(2,1)S(1)} copy(bf16[1,4096,128]{2,1,0:T(8,128)(2,1)S(1)} %add_convert_fusion) | data formatting | bytes 2097152 | tf_op jit(solution)/shard_map/convert_element_type | solution.py:77
  306.1 22.4 %reduce.20 = bf16[4096,128]{1,0:T(8,128)(2,1)S(1)} reduce(bf16[4096,1,128]{2,1,0:T(2,128)(2,1)S(1)} %bitcast.227, bf16[]{:T(256)} %broadcast.202), dimensions={1}, to_apply=%bitcast.205.reduce_sub_computation | reduce | bytes 2097154
  329.6 3.7 all-to-all-start.3
  334.0 13.9 %psum.35 = f32[2048]{0:T(1024)S(1)} all-reduce(f32[2048]{0:T(1024)S(1)} %get-tuple-element.40), channel_id=1, replica_groups=mesh['sp_0'=4,'sp_1'=4,'dp_0'=8,'dp_1'=2] {'sp_0'}, use_global_device_ids=true, to_apply=%region_39.40 | all-reduce | flops 2048 | bytes 16384 | tf_op jit(solution)/shard_map/psum | solution.py:26
  348.0 13.8 %psum.36 = f32[2048]{0:T(1024)S(1)} all-reduce(f32[2048]{0:T(1024)S(1)} %psum.35), channel_id=1, replica_groups=mesh['sp_0'=4,'sp_1'=4,'dp_0'=8,'dp_1'=2] {'sp_1'}, use_global_device_ids=true, to_apply=%region_40.41 | all-reduce | flops 2048 | bytes 16384 | tf_op jit(solution)/shard_map/psum | solution.py:26
  361.8 15.9 %psum.37 = f32[2048]{0:T(1024)S(1)} all-reduce(f32[2048]{0:T(1024)S(1)} %psum.36), channel_id=1, replica_groups=mesh['sp_0'=4,'sp_1'=4,'dp_0'=8,'dp_1'=2] {'dp_0'}, use_global_device_ids=true, to_apply=%region_41.42 | all-reduce | flops 2048 | bytes 16384 | tf_op jit(solution)/shard_map/psum | solution.py:26
  377.7 3.1 psum.38
  382.6 1.5 convert_bitcast_fusion
  384.1 3.1 copy.89
  387.2 3.4 fusion.4
  390.6 2.3 copy.93
  394.3 42.0 %all-reduce.4.cloned.1.call-done = f32[128,2048]{0,1:T(8,128)} async-done(((f32[128,2048]{0,1:T(8,128)}), f32[128,2048]{0,1:T(8,128)}) %all-reduce.4.cloned.1.call-update) | async-done | bytes 1048592 | tf_op jit(solution)/shard_map/psum | solution.py:91
  436.3 2.5 copy.94
  (56 shorter events, 14.3 us)
Async XLA Ops:
  7.2 156.7 %copy-start = (bf16[1,256,2048]{2,1,0:T(8,128)(2,1)S(1)}, bf16[1,256,2048]{2,1,0:T(8,128)(2,1)}, u32[]{:S(2)}) copy-start(bf16[1,256,2048]{2,1,0:T(8,128)(2,1)} %param.8) | copy-start | bytes 3145732
  7.2 170.2 %all-gather.2.cloned.1.call-start = ((), (), s32[]{:S(2)}) async-start(), calls=%async_computation.6 | async-start | bytes 8912896 | tf_op jit(solution)/shard_map/all_gather | solution.py:54
  9.4 2.5 copy-start.5
  11.3 13.5 %copy-start.7 = (bf16[1,256,2048]{1,2,0:T(8,128)(2,1)}, bf16[1,256,2048]{1,2,0:T(8,128)(2,1)S(1)}, u32[]{:S(2)}) copy-start(bf16[1,256,2048]{1,2,0:T(8,128)(2,1)S(1)} %copy.76) | copy-start | bytes 3145732
  37.0 8.4 %copy-start.11 = (f32[31,128]{1,0:T(8,128)S(1)}, f32[31,128]{1,0:T(8,128)}, u32[]{:S(2)}) copy-start(f32[31,128]{1,0:T(8,128)} %param.9) | copy-start | bytes 47620
  38.1 24.8 %all-to-all-start = ((bf16[16,2,16384]{2,1,0:T(2,128)(2,1)}), bf16[16,2,16384]{2,1,0:T(2,128)(2,1)}, u32[]{:S(2)}, u32[]{:S(2)}) async-start(bf16[16,2,16384]{2,1,0:T(2,128)(2,1)} %reshape.390), calls=%async_computation | async-start | bytes 2097152 | tf_op jit(solution)/shard_map/all_to_all | solution.py:34
  45.2 288.2 %reduce-scatter.2.cloned.1.call-start = ((), (), s32[]{:S(2)}) async-start(), calls=%async_computation.7 | async-start | bytes 17825792 | tf_op jit(solution)/shard_map/reduce_scatter | solution.py:83
  67.2 2.0 copy-start.4
  157.6 2.1 copy-start.10
  157.6 2.2 copy-start.3
  177.4 7.7 %copy-start.9 = (f32[1,256,16,128]{3,2,1,0:T(8,128)S(1)}, f32[1,256,16,128]{3,2,1,0:T(8,128)}, u32[]{:S(2)}) copy-start(f32[1,256,16,128]{3,2,1,0:T(8,128)} %copy.83) | copy-start | bytes 6291460
  231.4 3.0 copy-start.2
  243.6 86.0 %all-to-all-start.4 = ((f32[16,31,128]{2,1,0:T(8,128)}), f32[16,31,128]{2,1,0:T(8,128)S(1)}, u32[]{:S(2)}, u32[]{:S(2)}) async-start(f32[16,31,128]{2,1,0:T(8,128)} %broadcast_in_dim.2), calls=%async_computation.4 | async-start | bytes 524288 | tf_op jit(solution)/shard_map/all_to_all | solution.py:16
  329.6 51.8 %all-to-all-start.3 = ((bf16[16,2,16384]{2,1,0:T(2,128)(2,1)}), bf16[16,2,16384]{2,1,0:T(2,128)(2,1)S(1)}, u32[]{:S(2)}, u32[]{:S(2)}) async-start(bf16[16,2,16384]{2,1,0:T(2,128)(2,1)} %reshape.396), calls=%async_computation.3 | async-start | bytes 2097152 | tf_op jit(solution)/shard_map/all_to_all | solution.py:76
  333.3 103.0 %all-reduce.4.cloned.1.call-start = ((), (), s32[]{:S(2)}) async-start(), calls=%async_computation.8 | async-start | bytes 2097152 | tf_op jit(solution)/shard_map/psum | solution.py:91
  384.1 3.1 copy-start.6
  384.1 3.1 copy-start.8
  392.9 45.9 %copy-start.1 = (bf16[1,256,2048]{2,1,0:T(8,128)(2,1)S(1)}, bf16[1,256,2048]{2,1,0:T(8,128)(2,1)}, u32[]{:S(2)}) copy-start(bf16[1,256,2048]{2,1,0:T(8,128)(2,1)} %param.8) | copy-start | bytes 3145732
Sparse Core Ops, SparseCore 0:
  9.8 56.6 all-gather.1
  173.3 101.6 reduce-scatter.1
  337.3 98.8 all-reduce.3
where the time goes:
time: 452 us; the launch traced here: 446 us
  other arithmetic  148 us (33%)
  local copies, waits for them, and re-layouts  99.6 us (22%)
  blocking collectives  85.9 us (19%)
  waiting for transfers between devices  60.8 us (13%)
  starting transfers between devices  19.5 us (4%)
  matrix products  17 us (4%)
  between operations  14.2 us (3%)
    unnamed x4, other arithmetic  70.5 us
    psum x4, blocking collectives, one_axis_at_a_time(): return functools.reduce(lax.psum, axes, shard)  46.7 us
    psum x1, waiting for transfers between devices, body(): grad_weight = lax.psum(owned, SP)  42 us
    convert_element_type x1, other arithmetic, body(): grad_glu.astype(jnp.bfloat16)  37.3 us
    unnamed x38, local copies, waits for them, and re-layouts  30.8 us
    all_to_all x1, blocking collectives, body(): lax.all_to_all(conv_out.astype(jnp.bfloat16), SP, split_axis=1, concat_ax...  20.4 us
    all_to_all x1, blocking collectives, body(): lax.all_to_all(grad_conv_out.astype(jnp.bfloat16), SP, split_axis=2, conc...  18.8 us
    all_to_all x1, waiting for transfers between devices, body(): lax.all_to_all(glu, SP, split_axis=2, concat_axis=1, tiled=True)  17.5 us
  transfers between devices with their start and end apart: 6, of which 2 were waited for; matrix products, arithmetic and copies ran while one was open for 59% of the time, Pallas kernels for 0%

commit v1 on v0

--- a/solution.py
+++ b/solution.py
@@ -88,7 +88,11 @@
         scatter_dimension=0,
         tiled=True,
     )
-    grad_weight = lax.psum(owned, SP)
+
+    def counts_feed(z, mesh_name):
+        return lax.all_gather(z, axis_name=mesh_name).sum(axis=0)
+
+    grad_weight = counts_feed(owned, SP)
     return (grad_value, grad_gate, grad_taps, grad_gain, grad_weight)
 
 

time: 452 us -> 589 us (1.30)
  waiting for transfers between devices: 60.8 us -> 167 us
  other arithmetic: 148 us -> 159 us
  blocking collectives: 85.9 us -> 94.9 us
  local copies, waits for them, and re-layouts: 99.6 us -> 108 us
    reduce_scatter x1, waiting for transfers between devices: 0.02 us -> 95.5 us  [body(): lax.psum_scatter(lax.dot_general(columns, activated, (((0,), (0,)), ((),...]
    all_gather x1, waiting for transfers between devices: 0.01 us -> 53.7 us  [body(): lax.all_gather(out_weight, DP, axis=0, tiled=True)]
    psum x1 -> x0, waiting for transfers between devices: 42 us -> none  [body(): grad_weight = lax.psum(owned, SP)]
    reduce_sum x0 -> x1, other arithmetic: none -> 11.9 us  [counts_feed(): return lax.all_gather(z, axis_name=mesh_name).sum(axis=0)]
    all_to_all x1, blocking collectives: 18.8 us -> 27.3 us  [body(): lax.all_to_all(grad_conv_out.astype(jnp.bfloat16), SP, split_axis=2, conc...]
    unnamed x38 -> x41, local copies, waits for them, and re-layouts: 30.8 us -> 39.1 us
  transfers between devices with their start and end apart: 6 -> 6, of which waited for: 2 -> 3; matrix products, arithmetic and copies ran while one was open for 59% -> 24% of each run, Pallas kernels for 0% -> 0%
where the time goes in v1:
time: 589 us; the launch traced here: 580 us
  waiting for transfers between devices  167 us (28%)
  other arithmetic  159 us (27%)
  local copies, waits for them, and re-layouts  108 us (18%)
  blocking collectives  94.9 us (16%)
  starting transfers between devices  19.8 us (3%)
  matrix products  17 us (3%)
  between operations  14.3 us (2%)
    reduce_scatter x1, waiting for transfers between devices, body(): lax.psum_scatter(lax.dot_general(columns, activated, (((0,), (0,)), ((),...  95.5 us
    unnamed x4, other arithmetic  70.1 us
    all_gather x1, waiting for transfers between devices, body(): lax.all_gather(out_weight, DP, axis=0, tiled=True)  53.7 us
    psum x4, blocking collectives, one_axis_at_a_time(): return functools.reduce(lax.psum, axes, shard)  47.5 us
    unnamed x41, local copies, waits for them, and re-layouts  39.1 us
    convert_element_type x1, other arithmetic, body(): grad_glu.astype(jnp.bfloat16)  37.3 us
    all_to_all x1, blocking collectives, body(): lax.all_to_all(grad_conv_out.astype(jnp.bfloat16), SP, split_axis=2, conc...  27.3 us
    all_to_all x1, blocking collectives, body(): lax.all_to_all(conv_out.astype(jnp.bfloat16), SP, split_axis=1, concat_ax...  20.2 us
  transfers between devices with their start and end apart: 6, of which 3 were waited for; matrix products, arithmetic and copies ran while one was open for 24% of the time, Pallas kernels for 0%

profile of v1, /device:TPU:32, one launch (start us, length us, event | category | flops | bytes accessed | tf_op | source)
XLA Modules:
  0.0 579.8 jit_solution(15061841898495327684)
XLA Ops:
  8.8 1.9 copy.73
  11.2 12.9 %copy.118 = bf16[1,256,2048]{1,0,2:T(2,128)(2,1)} copy(bf16[1,256,2048]{1,2,0:T(8,128)(2,1)S(1)} %fusion.1) | data formatting | bytes 2097152 | tf_op jit(solution)/shard_map/convert_element_type | solution.py:33
  24.7 11.6 %reduce.17 = bf16[2048,256]{1,0:T(8,128)(2,1)S(1)} reduce(bf16[2048,1,256]{2,1,0:T(2,128)(2,1)} %bitcast.232, bf16[]{:T(256)} %broadcast.202), dimensions={1}, to_apply=%bitcast.212.reduce_sub_computation | reduce | bytes 2097154
  37.4 7.1 %all-to-all-start = ((bf16[16,2,16384]{2,1,0:T(2,128)(2,1)}), bf16[16,2,16384]{2,1,0:T(2,128)(2,1)}, u32[]{:S(2)}, u32[]{:S(2)}) async-start(bf16[16,2,16384]{2,1,0:T(2,128)(2,1)} %reshape.391), calls=%async_computation | async-start | bytes 2097152 | tf_op jit(solution)/shard_map/all_to_all | solution.py:34
  44.8 17.5 %all-to-all-done = bf16[16,2,16384]{2,1,0:T(2,128)(2,1)} async-done(((bf16[16,2,16384]{2,1,0:T(2,128)(2,1)}), bf16[16,2,16384]{2,1,0:T(2,128)(2,1)}, u32[]{:S(2)}, u32[]{:S(2)}) %all-to-all-start) | async-done | bytes 1048608 | tf_op jit(solution)/shard_map/all_to_all | solution.py:34
  62.3 4.3 reshape.392
  66.6 1.6 copy_convert_fusion.2
  68.5 1.9 copy.76
  70.4 8.6 %add_convert_fusion.1 = bf16[1,4096,128]{2,1,0:T(8,128)(2,1)S(1)} fusion(f32[128]{0:T(128)S(1)} %get-tuple-element.89, f32[128]{0:T(128)S(1)} %get-tuple-element.90, f32[128]{0:T(128)S(1)} %get-tuple-element.61, f32[128]{0:T(128)S(1)} %get-tuple-element.62, f32[128]{0:T(128)S(1)} %get-tuple-element.63, f32[128]{0:T(128)S(1)} %get-tuple-element.64, ...), kind=kLoop, calls=%fused_computation.84 | loop fusion | flops 32505856 | bytes 5258752 | tf_op jit(solution)/shard_map/convert_element_type | solution.py:41
  79.0 17.1 %copy.117 = bf16[1,4096,128]{2,0,1:T(2,128)(2,1)} copy(bf16[1,4096,128]{2,1,0:T(8,128)(2,1)S(1)} %add_convert_fusion.1) | data formatting | bytes 2097152 | tf_op jit(solution)/shard_map/convert_element_type | solution.py:41
  96.1 24.4 %reduce.18 = bf16[4096,128]{1,0:T(8,128)(2,1)} reduce(bf16[4096,1,128]{2,1,0:T(2,128)(2,1)} %bitcast.234, bf16[]{:T(256)} %broadcast.202), dimensions={1}, to_apply=%bitcast.211.reduce_sub_computation | reduce | bytes 2097154
  120.5 2.1 reshape.393
  122.6 20.2 %all_to_all.20 = bf16[16,2,16384]{2,1,0:T(2,128)(2,1)} all-to-all(bf16[16,2,16384]{2,1,0:T(2,128)(2,1)} %reshape.393), channel_id=1, replica_groups=mesh['sp_0'=4,'sp_1'=4,'dp_0'=8,'dp_1'=2] {'sp_0','sp_1'}, dimensions={0} | all-to-all | bytes 2097152 | tf_op jit(solution)/shard_map/all_to_all | solution.py:40
  142.7 5.8 reshape.394
  148.5 2.4 fusion.33
  152.4 2.9 copy.79
  155.3 2.0 fusion.11
  157.6 1.8 fusion.29
  159.4 2.3 copy.88
  161.6 9.3 %convolution_bitcast_fusion = f32[2048,2048]{0,1:T(8,128)} fusion(bf16[256,2048]{0,1:T(8,128)(2,1)} %bitcast.239, bf16[1,256,2048]{2,1,0:T(8,128)(2,1)S(1)} %copy-done), kind=kOutput, calls=%fused_computation.1 | convolution fusion | flops 2147483648 | bytes 18874368 | tf_op jit(solution)/shard_map/dot_general | solution.py:84
  171.7 95.5 %reduce-scatter.2.cloned.1.call-done = f32[128,2048]{0,1:T(8,128)} async-done(((f32[2048,2048]{0,1:T(8,128)}), f32[128,2048]{0,1:T(8,128)}) %reduce-scatter.2.cloned.1.call-update) | async-done | bytes 1048592 | tf_op jit(solution)/shard_map/reduce_scatter | solution.py:83
  267.3 4.2 copy.80
  271.5 53.7 %all-gather.4.cloned.1.call-done = bf16[2048,2048]{1,0:T(8,128)(2,1)} async-done(((bf16[128,2048]{1,0:T(8,128)(2,1)}), bf16[2048,2048]{1,0:T(8,128)(2,1)}) %all-gather.4.cloned.1.call-update) | async-done | bytes 8388624 | tf_op jit(solution)/shard_map/all_gather | solution.py:54
  325.1 7.7 %multiply_reduce_fusion = (f32[2048]{0:T(1024)S(1)}, f32[256]{0:T(256)S(1)}, f32[256]{0:T(256)S(1)}, f32[256,2048]{1,0:T(8,128)S(1)}) fusion(f32[256]{0:T(256)S(1)} %add_rsqrt_fusion, f32[256]{0:T(256)S(1)} %broadcast_multiply_fusion.2, f32[32,8,16,128]{3,2,1,0:T(8,128)} %bitcast.230, f32[2048]{0:T(1024)S(1)} %copy-done.11, ...), kind=kOutput, calls=%fused_computation.23 | convolution fusion | flops 2156393984 | bytes 13651968 | tf_op jit(solution)/shard_map/dot_general | solution.py:52
  333.9 3.8 copy.81
  337.7 11.6 %reduce.19 = bf16[2048,256]{1,0:T(8,128)(2,1)S(1)} reduce(bf16[2048,1,256]{2,1,0:T(2,128)(2,1)} %bitcast.235, bf16[]{:T(256)} %broadcast.202), dimensions={1}, to_apply=%bitcast.199.reduce_sub_computation | reduce | bytes 2097154
  350.4 27.3 %all_to_all.42 = bf16[16,2,16384]{2,1,0:T(2,128)(2,1)S(1)} all-to-all(bf16[16,2,16384]{2,1,0:T(2,128)(2,1)} %reshape.395), channel_id=1, replica_groups=mesh['sp_0'=4,'sp_1'=4,'dp_0'=8,'dp_1'=2] {'sp_0','sp_1'}, dimensions={0} | all-to-all | bytes 2097152 | tf_op jit(solution)/shard_map/all_to_all | solution.py:65
  377.7 3.5 reshape.396
  381.2 3.1 copy_convert_fusion
  384.2 2.9 copy.83
  387.1 2.9 multiply_reduce_fusion.1
  391.0 2.5 multiply_reduce_fusion.2
  393.6 2.5 multiply_reduce_fusion.4
  396.1 2.5 multiply_reduce_fusion.3
  399.4 7.7 %all-to-all-start.4 = ((f32[16,31,128]{2,1,0:T(8,128)}), f32[16,31,128]{2,1,0:T(8,128)S(1)}, u32[]{:S(2)}, u32[]{:S(2)}) async-start(f32[16,31,128]{2,1,0:T(8,128)} %broadcast_in_dim.2), calls=%async_computation.4 | async-start | bytes 524288 | tf_op jit(solution)/shard_map/all_to_all | solution.py:16
  407.1 37.3 %add_convert_fusion = bf16[1,4096,128]{2,1,0:T(8,128)(2,1)S(1)} fusion(f32[1,4096,128]{2,1,0:T(8,128)} %bitcast.218, f32[128]{0:T(128)S(1)} %get-tuple-element.89, f32[128]{0:T(128)S(1)} %get-tuple-element.90, f32[128]{0:T(128)S(1)} %get-tuple-element.61, f32[128]{0:T(128)S(1)} %get-tuple-element.62, f32[128]{0:T(128)S(1)} %get-tuple-element.63, ...), kind=kLoop, calls=%fused_computation.55 | loop fusion | flops 32505856 | bytes 3161600 | tf_op jit(solution)/shard_map/convert_element_type | solution.py:77
  444.4 16.7 %copy.116 = bf16[1,4096,128]{2,0,1:T(2,128)(2,1)S(1)} copy(bf16[1,4096,128]{2,1,0:T(8,128)(2,1)S(1)} %add_convert_fusion) | data formatting | bytes 2097152 | tf_op jit(solution)/shard_map/convert_element_type | solution.py:77
  461.2 22.4 %reduce.20 = bf16[4096,128]{1,0:T(8,128)(2,1)S(1)} reduce(bf16[4096,1,128]{2,1,0:T(2,128)(2,1)S(1)} %bitcast.233, bf16[]{:T(256)} %broadcast.202), dimensions={1}, to_apply=%bitcast.210.reduce_sub_computation | reduce | bytes 2097154
  484.7 4.7 all-to-all-start.3
  489.4 14.3 %psum.28 = f32[2048]{0:T(1024)S(1)} all-reduce(f32[2048]{0:T(1024)S(1)} %get-tuple-element.25), channel_id=1, replica_groups=mesh['sp_0'=4,'sp_1'=4,'dp_0'=8,'dp_1'=2] {'sp_0'}, use_global_device_ids=true, to_apply=%region_39.40 | all-reduce | flops 2048 | bytes 16384 | tf_op jit(solution)/shard_map/psum | solution.py:26
  503.7 14.0 %psum.29 = f32[2048]{0:T(1024)S(1)} all-reduce(f32[2048]{0:T(1024)S(1)} %psum.28), channel_id=1, replica_groups=mesh['sp_0'=4,'sp_1'=4,'dp_0'=8,'dp_1'=2] {'sp_1'}, use_global_device_ids=true, to_apply=%region_40.41 | all-reduce | flops 2048 | bytes 16384 | tf_op jit(solution)/shard_map/psum | solution.py:26
  517.7 15.9 %psum.30 = f32[2048]{0:T(1024)S(1)} all-reduce(f32[2048]{0:T(1024)S(1)} %psum.29), channel_id=1, replica_groups=mesh['sp_0'=4,'sp_1'=4,'dp_0'=8,'dp_1'=2] {'dp_0'}, use_global_device_ids=true, to_apply=%region_41.42 | all-reduce | flops 2048 | bytes 16384 | tf_op jit(solution)/shard_map/psum | solution.py:26
  533.6 3.3 psum.31
  540.2 3.1 copy.86
  543.3 3.4 fusion.4
  546.7 2.3 copy.90
  550.4 9.4 %copy.94 = f32[256,8,16,128]{3,2,1,0:T(8,128)S(1)} copy(f32[256,8,16,128]{3,1,2,0:T(8,128)} %bitcast.228) | data formatting | bytes 33554432
  559.8 11.9 %bitcast_reduce_fusion = f32[128,2048]{0,1:T(8,128)S(1)} fusion(f32[256,8,16,128]{3,2,1,0:T(8,128)S(1)} %copy.94), kind=kLoop, calls=%fused_computation | loop fusion | flops 3932160 | bytes 17825792 | tf_op jit(solution)/shard_map/reduce_sum | solution.py:93
  (60 shorter events, 18.0 us)
Async XLA Ops:
  7.2 154.5 %copy-start = (bf16[1,256,2048]{2,1,0:T(8,128)(2,1)S(1)}, bf16[1,256,2048]{2,1,0:T(8,128)(2,1)}, u32[]{:S(2)}) copy-start(bf16[1,256,2048]{2,1,0:T(8,128)(2,1)} %param.8) | copy-start | bytes 3145732
  8.8 2.5 copy-start.6
  10.6 13.5 %copy-start.8 = (bf16[1,256,2048]{1,2,0:T(8,128)(2,1)}, bf16[1,256,2048]{1,2,0:T(8,128)(2,1)S(1)}, u32[]{:S(2)}) copy-start(bf16[1,256,2048]{1,2,0:T(8,128)(2,1)S(1)} %copy.73) | copy-start | bytes 3145732
  36.3 8.4 %copy-start.12 = (f32[31,128]{1,0:T(8,128)S(1)}, f32[31,128]{1,0:T(8,128)}, u32[]{:S(2)}) copy-start(f32[31,128]{1,0:T(8,128)} %param.9) | copy-start | bytes 47620
  37.4 24.8 %all-to-all-start = ((bf16[16,2,16384]{2,1,0:T(2,128)(2,1)}), bf16[16,2,16384]{2,1,0:T(2,128)(2,1)}, u32[]{:S(2)}, u32[]{:S(2)}) async-start(bf16[16,2,16384]{2,1,0:T(2,128)(2,1)} %reshape.391), calls=%async_computation | async-start | bytes 2097152 | tf_op jit(solution)/shard_map/all_to_all | solution.py:34
  44.5 222.7 %reduce-scatter.2.cloned.1.call-start = ((), (), s32[]{:S(2)}) async-start(), calls=%async_computation.7 | async-start | bytes 17825792 | tf_op jit(solution)/shard_map/reduce_scatter | solution.py:83
  66.6 2.0 copy-start.4
  148.5 2.4 copy-start.5
  152.4 5.0 copy-start.11
  155.3 2.2 copy-start.3
  170.9 154.2 %all-gather.4.cloned.1.call-start = ((), (), s32[]{:S(2)}) async-start(), calls=%async_computation.6 | async-start | bytes 8912896 | tf_op jit(solution)/shard_map/all_gather | solution.py:54
  171.7 378.7 %all-gather.6.cloned.1.call-start = ((), (), s32[]{:S(2)}) async-start(), calls=%async_computation.8 | async-start | bytes 17825792 | tf_op jit(solution)/shard_map/all_gather | solution.py:93
  325.1 7.7 %copy-start.10 = (f32[1,256,16,128]{3,2,1,0:T(8,128)S(1)}, f32[1,256,16,128]{3,2,1,0:T(8,128)}, u32[]{:S(2)}) copy-start(f32[1,256,16,128]{3,2,1,0:T(8,128)} %copy.80) | copy-start | bytes 6291460
  387.1 3.1 copy-start.2
  399.4 85.3 %all-to-all-start.4 = ((f32[16,31,128]{2,1,0:T(8,128)}), f32[16,31,128]{2,1,0:T(8,128)S(1)}, u32[]{:S(2)}, u32[]{:S(2)}) async-start(f32[16,31,128]{2,1,0:T(8,128)} %broadcast_in_dim.2), calls=%async_computation.4 | async-start | bytes 524288 | tf_op jit(solution)/shard_map/all_to_all | solution.py:16
  484.7 52.8 %all-to-all-start.3 = ((bf16[16,2,16384]{2,1,0:T(2,128)(2,1)}), bf16[16,2,16384]{2,1,0:T(2,128)(2,1)S(1)}, u32[]{:S(2)}, u32[]{:S(2)}) async-start(bf16[16,2,16384]{2,1,0:T(2,128)(2,1)} %reshape.397), calls=%async_computation.3 | async-start | bytes 2097152 | tf_op jit(solution)/shard_map/all_to_all | solution.py:76
  540.2 3.1 copy-start.7
  540.2 3.1 copy-start.9
  559.8 13.2 %copy-start.1 = (bf16[1,256,2048]{2,1,0:T(8,128)(2,1)S(1)}, bf16[1,256,2048]{2,1,0:T(8,128)(2,1)}, u32[]{:S(2)}) copy-start(bf16[1,256,2048]{2,1,0:T(8,128)(2,1)} %param.8) | copy-start | bytes 3145732
Sparse Core Ops, SparseCore 0:
  171.1 96.1 reduce-scatter.1
  269.1 55.9 all-gather.3
  327.5 136.0 all-gather.5
